TPU v7x, 32 devices: a whole 2x2x4 slice. The times are simulated.
32 devices in a mesh: rep: 2 (over x), fs: 8 (over z, y), tp: 2 (over core).
Axes of the slice: x: 2, y: 2, z: 4, core: 2. Of those that a mesh axis runs over, the one named last changes fastest.
Arguments:
- tokens: bfloat16 [16, 512, 2048], P(('rep', 'fs'), 'tp'), may hold values from -6 to 6
- norm_first: bfloat16 [2048], replicated, may hold values from 0.099609375 to 1.8984375
- norm_mixer: bfloat16 [2048], replicated, may hold values from 0.099609375 to 1.8984375
- norm_second: bfloat16 [2048], replicated, may hold values from 0.099609375 to 1.8984375
- ffn_gate: bfloat16 [2048, 2816], P('fs', 'tp'), may hold values from -0.125 to 0.125
- ffn_up: bfloat16 [2048, 2816], P('fs', 'tp'), may hold values from -0.125 to 0.125
- ffn_down: bfloat16 [2816, 2048], P('tp', 'fs'), may hold values from -0.109375 to 0.109375
- conv_value: bfloat16 [2048, 512], P('fs', 'tp'), may hold values from -0.125 to 0.125
- conv_gate: bfloat16 [2048, 512], P('fs', 'tp'), may hold values from -0.125 to 0.125
- depthwise: bfloat16 [31, 512], P(None, 'tp'), may hold values from -1.5 to 1.5
- conv_gain: bfloat16 [512], P('tp'), may hold values from 0.099609375 to 1.8984375
- conv_out: bfloat16 [512, 2048], P('tp', 'fs'), may hold values from -0.25 to 0.25
Outputs:
- mixed: bfloat16 [16, 512, 2048], P(('rep', 'fs'), 'tp')
All inputs are finite; a program needn't handle non-finite values.
Results may differ from a plain program's by a relative error of at most 0.0095.
Values may be sent and summed in bfloat16 or wider, within the bound.
A program may use at most 128 MiB of HBM per device.

v0:
```python
import jax
import jax.numpy as jnp
from jax import lax
from jax.sharding import PartitionSpec as P

ROW_EPS = 0.05
CHAN_EPS = 0.02


def rms_rows(stream, gain_vec):
    square_mean = jnp.mean(stream * stream, axis=-1, keepdims=True)
    return (stream * lax.rsqrt(square_mean + ROW_EPS) * gain_vec.astype(jnp.float32)).astype(
        jnp.bfloat16
    )


def widen(normed):
    return lax.all_gather(normed, "tp", axis=0, tiled=True)


def narrow(partial_value):
    return lax.psum_scatter(
        partial_value.astype(jnp.bfloat16), "tp", scatter_dimension=0, tiled=True
    ).astype(jnp.float32)


def add_pair(gathered, portions):
    return (
        jnp.dot(gathered, portions[0], preferred_element_type=jnp.float32),
        jnp.dot(gathered, portions[1], preferred_element_type=jnp.float32),
    )


def hidden_units(gathered, whole_gate, whole_up):
    gate_rows = jnp.dot(gathered, whole_gate, preferred_element_type=jnp.float32)
    up_rows = jnp.dot(gathered, whole_up, preferred_element_type=jnp.float32)
    return (jax.nn.silu(gate_rows) * up_rows).astype(jnp.bfloat16)


def causal_taps(glu, kernel):
    length = glu.shape[0]
    taps = kernel.shape[0]
    padded = jnp.pad(glu, ((taps - 1, 0), (0, 0)))
    output = jnp.zeros_like(glu)
    for tap_index in range(taps):
        output = output + padded[tap_index : tap_index + length] * kernel[tap_index]
    return output


def shards(
    tokens,
    norm_first,
    norm_mixer,
    norm_second,
    ffn_gate,
    ffn_up,
    ffn_down,
    conv_value,
    conv_gate,
    depthwise,
    conv_gain,
    conv_out,
):
    width = tokens.shape[-1]
    stream = tokens.reshape(-1, width).astype(jnp.float32)
    first_rows = widen(rms_rows(stream, norm_first))
    whole_gate, whole_up, whole_down = (
        lax.all_gather(ffn_gate, "fs", axis=0, tiled=True),
        lax.all_gather(ffn_up, "fs", axis=0, tiled=True),
        lax.all_gather(ffn_down, "fs", axis=1, tiled=True),
    )
    hidden = hidden_units(first_rows, whole_gate, whole_up)
    first_out = jnp.dot(hidden, whole_down, preferred_element_type=jnp.float32)
    stream = stream + 0.5 * narrow(first_out)
    gathered = widen(rms_rows(stream, norm_mixer))
    values, gates = add_pair(
        gathered,
        (
            lax.all_gather(conv_value, "fs", axis=0, tiled=True),
            lax.all_gather(conv_gate, "fs", axis=0, tiled=True),
        ),
    )
    glu = values * jax.nn.sigmoid(gates)
    conv = causal_taps(glu, depthwise.astype(jnp.float32))
    channels = conv.shape[1] * lax.axis_size("tp")
    sums, squares = lax.psum((jnp.sum(conv, axis=1), jnp.sum(conv * conv, axis=1)), "tp")
    average = sums / channels
    spread = jnp.maximum(squares / channels - average * average, 0.0)
    centred = conv - average[:, None]
    activated = jax.nn.silu(
        centred * lax.rsqrt(spread[:, None] + CHAN_EPS) * conv_gain.astype(jnp.float32)
    ).astype(jnp.bfloat16)
    stream = stream + narrow(
        jnp.dot(
            activated,
            lax.all_gather(conv_out, "fs", axis=1, tiled=True),
            preferred_element_type=jnp.float32,
        )
    )
    second_rows = widen(rms_rows(stream, norm_second))
    second_hidden = hidden_units(second_rows, whole_gate, whole_up)
    second_out = jnp.dot(second_hidden, whole_down, preferred_element_type=jnp.float32)
    stream = stream + 0.5 * narrow(second_out)
    return stream.astype(jnp.bfloat16).reshape(tokens.shape)


def solution(mesh):
    in_specs = (
        P(("rep", "fs"), "tp", None),
        P(),
        P(),
        P(),
        P("fs", "tp"),
        P("fs", "tp"),
        P("tp", "fs"),
        P("fs", "tp"),
        P("fs", "tp"),
        P(None, "tp"),
        P("tp"),
        P("tp", "fs"),
    )
    out_specs = P(("rep", "fs"), "tp", None)
    return jax.shard_map(shards, mesh=mesh, in_specs=in_specs, out_specs=out_specs, check_vma=False)
```

profile of v0, /device:TPU:0, one launch (start us, length us, event | category | flops | bytes accessed | tf_op | source)
XLA Modules:
  0.0 537.0 jit_solution(4358337792304684496)
XLA Ops:
  6.5 0.0 all-gather.10.cloned.1.call-start
  6.5 0.7 convert_element_type.64
  7.2 1.5 fusion.2
  8.7 2.5 fusion.4
  11.3 0.0 all-gather.10.cloned.1.call-update
  11.3 0.0 all-gather.12.cloned.1.call-start
  11.3 0.7 all-gather.12.cloned.1.call-update
  12.0 0.0 all-gather.14.cloned.1.call-start
  12.1 0.7 all-gather.14.cloned.1.call-update
  12.8 0.0 all-gather.16.cloned.1.call-start
  12.8 0.5 all-gather.16.cloned.1.call-update
  13.3 0.0 reduce-scatter.4.cloned.1.call-start
  13.4 11.3 %all-gather.10.cloned.1.call-done = bf16[512,2048]{1,0:T(8,128)(2,1)} async-done(((bf16[256,2048]{1,0:T(8,128)(2,1)}), bf16[512,2048]{1,0:T(8,128)(2,1)}) %all-gather.10.cloned.1.call-update) | async-done | bytes 2097168 | tf_op jit(solution)/shard_map/all_gather | solution.py:18
  24.7 0.0 copy-start.6
  24.7 95.7 %all-gather.12.cloned.1.call-done = bf16[2048,1408]{1,0:T(8,128)(2,1)} async-done(((bf16[256,1408]{1,0:T(8,128)(2,1)}), bf16[2048,1408]{1,0:T(8,128)(2,1)}) %all-gather.12.cloned.1.call-update) | async-done | bytes 5767184 | tf_op jit(solution)/shard_map/all_gather | solution.py:68
  120.4 8.2 %fusion.52 = f32[512,1408]{1,0:T(8,128)} fusion(bf16[512,2048]{1,0:T(8,128)(2,1)} %all-gather.10.cloned.1.call-done, bf16[2048,1408]{1,0:T(8,128)(2,1)} %all-gather.12.cloned.1.call-done), kind=kOutput, calls=%fused_computation.93 | convolution fusion | flops 2952790016 | bytes 10747904 | tf_op jit(solution)/shard_map/dot_general | solution.py:35
  128.7 84.5 %all-gather.14.cloned.1.call-done = bf16[2048,1408]{1,0:T(8,128)(2,1)} async-done(((bf16[256,1408]{1,0:T(8,128)(2,1)}), bf16[2048,1408]{1,0:T(8,128)(2,1)}) %all-gather.14.cloned.1.call-update) | async-done | bytes 5767184 | tf_op jit(solution)/shard_map/all_gather | solution.py:69
  213.1 93.2 %all-gather.16.cloned.1.call-done = bf16[1408,2048]{1,0:T(8,128)(2,1)} async-done(((bf16[1408,256]{1,0:T(8,128)(2,1)}), bf16[1408,2048]{1,0:T(8,128)(2,1)}) %all-gather.16.cloned.1.call-update) | async-done | bytes 5767184 | tf_op jit(solution)/shard_map/all_gather | solution.py:70
  306.4 0.0 copy-done.6
  306.4 13.2 %convolution_convert_fusion.2 = bf16[512,2048]{1,0:T(8,128)(2,1)} fusion(bf16[1408,2048]{1,0:T(8,128)(2,1)} %all-gather.16.cloned.1.call-done, bf16[512,2048]{1,0:T(8,128)(2,1)S(1)} %copy-done.6, bf16[2048,1408]{1,0:T(8,128)(2,1)} %all-gather.14.cloned.1.call-done, f32[512,1408]{1,0:T(8,128)} %fusion.52), kind=kOutput, calls=%fused_computation.9 | convolution fusion | flops 5910953984 | bytes 18612224 | tf_op jit(solution)/shard_map/dot_general | solution.py:73
  319.6 0.0 reduce-scatter.4.cloned.1.call-update
  319.6 0.0 all-gather.22.cloned.1.call-start
  319.7 0.5 all-gather.22.cloned.1.call-update
  320.2 0.0 all-gather.18.cloned.1.call-start
  320.3 0.0 copy-done.4
  320.3 7.4 %reduce-scatter.4.cloned.1.call-done = bf16[256,2048]{1,0:T(8,128)(2,1)} async-done(((bf16[512,2048]{1,0:T(8,128)(2,1)}), bf16[256,2048]{1,0:T(8,128)(2,1)}) %reduce-scatter.4.cloned.1.call-update) | async-done | bytes 1048592 | tf_op jit(solution)/shard_map/reduce_scatter | solution.py:22
  327.7 0.0 copy-done
  327.7 1.8 multiply_reduce_fusion.1
  329.5 0.0 copy-done.1
  329.6 0.0 copy-start.7
  329.6 0.0 copy-start.3
  329.6 1.4 multiply_convert_fusion.1
  331.0 0.0 all-gather.18.cloned.1.call-update
  331.1 0.0 all-gather.20.cloned.1.call-start
  331.1 0.7 all-gather.20.cloned.1.call-update
  331.8 0.0 all-gather.24.cloned.1.call-start
  331.8 0.7 all-gather.24.cloned.1.call-update
  332.5 0.0 reduce-scatter.6.cloned.1.call-start
  332.6 0.0 copy-done.7
  332.6 0.0 copy-done.3
  332.7 38.6 %all-gather.22.cloned.1.call-done = bf16[2048,256]{1,0:T(8,128)(2,1)} async-done(((bf16[256,256]{1,0:T(8,128)(2,1)}), bf16[2048,256]{1,0:T(8,128)(2,1)}) %all-gather.22.cloned.1.call-update) | async-done | bytes 1048592 | tf_op jit(solution)/shard_map/all_gather | solution.py:80
  371.3 10.9 %all-gather.18.cloned.1.call-done = bf16[512,2048]{1,0:T(8,128)(2,1)} async-done(((bf16[256,2048]{1,0:T(8,128)(2,1)}), bf16[512,2048]{1,0:T(8,128)(2,1)}) %all-gather.18.cloned.1.call-update) | async-done | bytes 2097168 | tf_op jit(solution)/shard_map/all_gather | solution.py:18
  382.1 2.6 fusion.7
  384.7 41.0 %all-gather.20.cloned.1.call-done = bf16[2048,256]{1,0:T(8,128)(2,1)} async-done(((bf16[256,256]{1,0:T(8,128)(2,1)}), bf16[2048,256]{1,0:T(8,128)(2,1)}) %all-gather.20.cloned.1.call-update) | async-done | bytes 1048592 | tf_op jit(solution)/shard_map/all_gather | solution.py:79
  425.8 2.6 convolution_multiply_fusion.2
  428.3 2.4 fusion.49
  430.7 2.5 all-reduce.1
  433.2 32.8 %all-gather.24.cloned.1.call-done = bf16[256,2048]{1,0:T(8,128)(2,1)} async-done(((bf16[256,256]{1,0:T(8,128)(2,1)}), bf16[256,2048]{1,0:T(8,128)(2,1)}) %all-gather.24.cloned.1.call-update) | async-done | bytes 1048592 | tf_op jit(solution)/shard_map/all_gather | solution.py:96
  465.9 3.4 convolution_convert_fusion
  469.3 0.0 reduce-scatter.6.cloned.1.call-update
  469.3 0.2 all-gather.26.cloned.1.call-start
  469.6 0.4 copy-done.5
  470.0 8.2 %reduce-scatter.6.cloned.1.call-done = bf16[256,2048]{1,0:T(8,128)(2,1)} async-done(((bf16[512,2048]{1,0:T(8,128)(2,1)}), bf16[256,2048]{1,0:T(8,128)(2,1)}) %reduce-scatter.6.cloned.1.call-update) | async-done | bytes 1048592 | tf_op jit(solution)/shard_map/reduce_scatter | solution.py:22
  478.2 1.9 multiply_reduce_fusion
  480.2 0.0 copy-done.2
  480.2 1.6 multiply_convert_fusion
  481.8 0.0 all-gather.26.cloned.1.call-update
  481.9 0.0 reduce-scatter.8.cloned.1.call-start
  481.9 12.0 %all-gather.26.cloned.1.call-done = bf16[512,2048]{1,0:T(8,128)(2,1)} async-done(((bf16[256,2048]{1,0:T(8,128)(2,1)}), bf16[512,2048]{1,0:T(8,128)(2,1)}) %all-gather.26.cloned.1.call-update) | async-done | bytes 2097168 | tf_op jit(solution)/shard_map/all_gather | solution.py:18
  493.9 8.2 %fusion.53 = f32[512,1408]{1,0:T(8,128)} fusion(bf16[512,2048]{1,0:T(8,128)(2,1)} %all-gather.26.cloned.1.call-done, bf16[2048,1408]{1,0:T(8,128)(2,1)} %all-gather.12.cloned.1.call-done), kind=kOutput, calls=%fused_computation.94 | convolution fusion | flops 2952790016 | bytes 10747904 | tf_op jit(solution)/shard_map/dot_general | solution.py:35
  502.1 13.9 %convolution_convert_fusion.1 = bf16[512,2048]{1,0:T(8,128)(2,1)} fusion(bf16[1408,2048]{1,0:T(8,128)(2,1)} %all-gather.16.cloned.1.call-done, bf16[512,2048]{1,0:T(8,128)(2,1)} %all-gather.26.cloned.1.call-done, bf16[2048,1408]{1,0:T(8,128)(2,1)} %all-gather.14.cloned.1.call-done, f32[512,1408]{1,0:T(8,128)} %fusion.53), kind=kOutput, calls=%fused_computation.8 | convolution fusion | flops 5910953984 | bytes 18612224 | tf_op jit(solution)/shard_map/dot_general | solution.py:102
  516.0 0.0 reduce-scatter.8.cloned.1.call-update
  516.1 11.1 %reduce-scatter.8.cloned.1.call-done = bf16[256,2048]{1,0:T(8,128)(2,1)} async-done(((bf16[512,2048]{1,0:T(8,128)(2,1)}), bf16[256,2048]{1,0:T(8,128)(2,1)}) %reduce-scatter.8.cloned.1.call-update) | async-done | bytes 1048592 | tf_op jit(solution)/shard_map/reduce_scatter | solution.py:22
  527.2 2.9 fusion.8
  (14 shorter events, 0.1 us)
Async XLA Ops:
  6.5 18.2 %all-gather.10.cloned.1.call-start = ((), (), s32[]{:S(2)}) async-start(), calls=%async_computation.3 | async-start | bytes 3145728 | tf_op jit(solution)/shard_map/all_gather | solution.py:18
  11.3 109.2 %all-gather.12.cloned.1.call-start = ((), (), s32[]{:S(2)}) async-start(), calls=%async_computation.4 | async-start | bytes 6488064 | tf_op jit(solution)/shard_map/all_gather | solution.py:68
  12.0 201.1 %all-gather.14.cloned.1.call-start = ((), (), s32[]{:S(2)}) async-start(), calls=%async_computation.5 | async-start | bytes 6488064 | tf_op jit(solution)/shard_map/all_gather | solution.py:69
  12.8 293.6 %all-gather.16.cloned.1.call-start = ((), (), s32[]{:S(2)}) async-start(), calls=%async_computation.6 | async-start | bytes 6488064 | tf_op jit(solution)/shard_map/all_gather | solution.py:70
  13.3 314.4 %reduce-scatter.4.cloned.1.call-start = ((), (), s32[]{:S(2)}) async-start(), calls=%async_computation.7 | async-start | bytes 3145728 | tf_op jit(solution)/shard_map/reduce_scatter | solution.py:22
  24.7 281.7 %copy-start.6 = (bf16[512,2048]{1,0:T(8,128)(2,1)S(1)}, bf16[512,2048]{1,0:T(8,128)(2,1)}, u32[]{:S(2)}) copy-start(bf16[512,2048]{1,0:T(8,128)(2,1)} %all-gather.10.cloned.1.call-done) | copy-start | bytes 6291460
  319.6 0.7 copy-start.4
  319.6 8.1 %copy-start = (bf16[1,256,2048]{2,1,0:T(8,128)(2,1)S(1)}, bf16[1,256,2048]{2,1,0:T(8,128)(2,1)}, u32[]{:S(2)}) copy-start(bf16[1,256,2048]{2,1,0:T(8,128)(2,1)} %param.12) | copy-start | bytes 3145732
  319.6 51.7 %all-gather.22.cloned.1.call-start = ((), (), s32[]{:S(2)}) async-start(), calls=%async_computation.10 | async-start | bytes 1179648 | tf_op jit(solution)/shard_map/all_gather | solution.py:80
  320.2 61.9 %all-gather.18.cloned.1.call-start = ((), (), s32[]{:S(2)}) async-start(), calls=%async_computation.8 | async-start | bytes 3145728 | tf_op jit(solution)/shard_map/all_gather | solution.py:18
  327.7 1.8 copy-start.1
  329.6 3.0 copy-start.7
  329.6 3.0 copy-start.3
  331.1 94.7 %all-gather.20.cloned.1.call-start = ((), (), s32[]{:S(2)}) async-start(), calls=%async_computation.9 | async-start | bytes 1179648 | tf_op jit(solution)/shard_map/all_gather | solution.py:79
  331.8 134.1 %all-gather.24.cloned.1.call-start = ((), (), s32[]{:S(2)}) async-start(), calls=%async_computation.11 | async-start | bytes 1179648 | tf_op jit(solution)/shard_map/all_gather | solution.py:96
  332.5 145.7 %reduce-scatter.6.cloned.1.call-start = ((), (), s32[]{:S(2)}) async-start(), calls=%async_computation.12 | async-start | bytes 3145728 | tf_op jit(solution)/shard_map/reduce_scatter | solution.py:22
  469.3 0.7 copy-start.5
  469.3 24.5 %all-gather.26.cloned.1.call-start = ((), (), s32[]{:S(2)}) async-start(), calls=%async_computation.13 | async-start | bytes 3145728 | tf_op jit(solution)/shard_map/all_gather | solution.py:18
  478.2 1.9 copy-start.2
  481.9 45.3 %reduce-scatter.8.cloned.1.call-start = ((), (), s32[]{:S(2)}) async-start(), calls=%async_computation.14 | async-start | bytes 3145728 | tf_op jit(solution)/shard_map/reduce_scatter | solution.py:22
Sparse Core Ops, SparseCore 0:
  11.4 13.2 all-gather.9
  26.9 93.4 all-gather.11
  122.6 90.4 all-gather.13
  215.0 91.2 all-gather.15
  319.8 7.9 reduce-scatter.3
  329.7 41.5 all-gather.21
  372.8 9.2 all-gather.17
  384.3 41.4 all-gather.19
  427.8 38.0 all-gather.23
  469.5 8.7 reduce-scatter.5
  482.0 11.8 all-gather.25
  516.2 10.9 reduce-scatter.7
where the time goes:
time: 537 us
  waiting for transfers between devices  451 us (84%)
  matrix products  52.1 us (10%)
  other arithmetic  16.9 us (3%)
  between operations  13.7 us (3%)
    all_gather x1, waiting for transfers between devices, shards(): lax.all_gather(ffn_gate, 'fs', axis=0, tiled=True)  95.7 us
    all_gather x1, waiting for transfers between devices, shards(): lax.all_gather(ffn_down, 'fs', axis=1, tiled=True)  93.2 us
    all_gather x1, waiting for transfers between devices, shards(): lax.all_gather(ffn_up, 'fs', axis=0, tiled=True)  84.5 us
    all_gather x1, waiting for transfers between devices, shards(): lax.all_gather(conv_value, 'fs', axis=0, tiled=True)  41 us
    all_gather x1, waiting for transfers between devices, shards(): lax.all_gather(conv_gate, 'fs', axis=0, tiled=True)  38.6 us
    all_gather x3, waiting for transfers between devices, widen(): return lax.all_gather(normed, 'tp', axis=0, tiled=True)  34.2 us
    all_gather x1, waiting for transfers between devices, shards(): lax.all_gather(conv_out, 'fs', axis=1, tiled=True)  32.8 us
    reduce_scatter x3, waiting for transfers between devices, narrow(): lax.psum_scatter(partial_value.astype(jnp.bfloat16), 'tp', scatter_dimens...  26.8 us
  transfers between devices with their start and end apart: 12, of which 12 were waited for; matrix products, arithmetic and copies ran while one was open for 4% of the time, Pallas kernels for 0%

commit v1 on v0

v1 whole, which is shorter than its diff:
```python
import functools

import jax
import jax.numpy as jnp
from jax import lax
from jax.experimental import pallas as pl
from jax.experimental.pallas import tpu as pltpu
from jax.sharding import PartitionSpec as P

ROW_EPS = 0.05
CHAN_EPS = 0.02
MESH = pl.DeviceIdType.MESH
LEAD = 1.5
LAG = 1.6


def rms_rows(stream, gain_vec):
    square_mean = jnp.mean(stream * stream, axis=-1, keepdims=True)
    return (stream * lax.rsqrt(square_mean + ROW_EPS) * gain_vec.astype(jnp.float32)).astype(
        jnp.bfloat16
    )


def swap(value):
    size = lax.axis_size("tp")
    return lax.ppermute(value, "tp", [(i, size - 1 - i) for i in range(size)])


def widen(normed):
    return jnp.concatenate([normed, swap(normed)])


def narrow(partial_value):
    rounded = partial_value.astype(jnp.bfloat16)
    half = rounded.shape[0] // 2
    return rounded[:half].astype(jnp.float32) + swap(rounded[half:]).astype(jnp.float32)


def reorder(rows):
    half = rows.shape[0] // 2
    flipped = jnp.concatenate([rows[half:], rows[:half]])
    return jnp.where(lax.axis_index("tp") == 0, rows, flipped)


def place():
    fs = lax.axis_index("fs")
    return lax.axis_index("rep"), lax.rem(fs, 2), fs // 2


class Gather:
    def __init__(self, depth, ins, slots, local_sems, recv_sems, send_sems):
        self.depth = depth
        self.ins, self.slots = ins, slots
        self.local_sems, self.recv_sems, self.send_sems = local_sems, recv_sems, send_sems
        self.x, self.y, self.z = place()

    def targets(self):
        other_x = {"rep": 1 - self.x}
        other_y = {"fs": self.z * 2 + 1 - self.y}
        up = {"fs": (self.z + 1) * 2 + self.y}
        down = {"fs": (self.z - 1) * 2 + self.y}
        return up, down, other_x, other_y

    def barrier(self):
        barrier = pltpu.get_barrier_semaphore()
        up, down, other_x, other_y = self.targets()
        has_up, has_down = self.z + 1 < self.depth, self.z > 0
        for target in (other_x, other_y):
            pl.semaphore_signal(barrier, inc=1, device_id=target, device_id_type=MESH)

        @pl.when(has_up)
        def _():
            pl.semaphore_signal(barrier, inc=1, device_id=up, device_id_type=MESH)

        @pl.when(has_down)
        def _():
            pl.semaphore_signal(barrier, inc=1, device_id=down, device_id_type=MESH)

        peers = 2 + has_up.astype(jnp.int32) + has_down.astype(jnp.int32)
        pl.semaphore_wait(barrier, peers)

    def local(self, m, c):
        k = self.z * 2 + self.y
        return pltpu.make_async_copy(
            self.ins[m].at[c], self.slots[m].at[k, c], self.local_sems[m].at[c]
        )

    def copy(self, m, c, k, way):
        piece = self.slots[m].at[k, c]
        return pltpu.make_async_remote_copy(
            src_ref=piece,
            dst_ref=piece,
            send_sem=self.send_sems[m].at[way, k, c],
            recv_sem=self.recv_sems[m].at[k, c],
            device_id=self.targets()[way],
            device_id_type=MESH,
        )

    def routes(self, m, c, side, d):
        x, y, z = self.x, self.y, self.z
        home = x == lax.rem(c, 2)
        has_up, has_down = z + 1 < self.depth, z > 0
        off = z < 0
        if side == "far_below":
            return (z - d) * 2 + 1 - y, z - d >= 0, (off, off, home, off)
        if side == "far_above":
            return (z + d) * 2 + 1 - y, z + d < self.depth, (off, off, home, off)
        if side == "own":
            return z * 2 + y, z >= 0, (has_up, has_down, off, home)
        if side == "below":
            return (z - d) * 2 + y, z - d >= 0, (has_up, off, off, home)
        return (z + d) * 2 + y, z + d < self.depth, (off, has_down, off, home)

    def event(self, m, side, d, finish=False):
        def step(c, carry):
            k, present, sends = self.routes(m, c, side, d)

            @pl.when(present)
            def _():
                if not finish:
                    if side == "own":
                        self.local(m, c).wait()
                    else:
                        self.copy(m, c, k, 2).wait_recv()
                for way, wanted in enumerate(sends):

                    @pl.when(wanted)
                    def _(way=way):
                        if finish:
                            self.copy(m, c, k, way).wait_send()
                        else:
                            self.copy(m, c, k, way).start()

            return carry

        lax.fori_loop(0, self.ins[m].shape[0], step, 0)

    def start_local(self):
        for m in range(len(self.ins)):

            def step(c, carry, m=m):
                self.local(m, c).start()
                return carry

            lax.fori_loop(0, self.ins[m].shape[0], step, 0)

    def plan(self):
        events = []
        span = self.depth - 1
        for m in range(len(self.ins)):
            start = m * span
            events.append((start - LEAD, m, "own", 0))
            events.append((start + LAG, m, "far_below", 0))
            for d in range(1, self.depth):
                events.append((start + d, m, "below", d))
                events.append((start + d, m, "above", d))
                events.append((start + d + LAG, m, "far_below", d))
                events.append((start + d + LAG, m, "far_above", d))
        return sorted(events, key=lambda event: event[0])

    def finish(self):
        for _, m, side, d in self.plan():
            self.event(m, side, d, finish=True)


def gather_kernel(depth, count, *refs):
    ins, slots = refs[:count], refs[count : 2 * count]
    sems = refs[2 * count :]
    gather = Gather(depth, ins, slots, sems[:count], sems[count : 2 * count], sems[2 * count :])
    gather.start_local()
    gather.barrier()
    for _, m, side, d in gather.plan():
        gather.event(m, side, d)
    gather.finish()


def gather_all(blocks):
    total = lax.axis_size("fs")
    count = len(blocks)
    outs = [jax.ShapeDtypeStruct((total, *b.shape), b.dtype) for b in blocks]
    dma = pltpu.SemaphoreType.DMA
    return pl.pallas_call(
        functools.partial(gather_kernel, total // 2, count),
        out_shape=outs,
        in_specs=[pl.BlockSpec(memory_space=pl.ANY)] * count,
        out_specs=[pl.BlockSpec(memory_space=pltpu.VMEM)] * count,
        scratch_shapes=[dma((b.shape[0],)) for b in blocks]
        + [dma((total, b.shape[0])) for b in blocks]
        + [dma((4, total, b.shape[0])) for b in blocks],
        compiler_params=pltpu.CompilerParams(
            collective_id=0, has_side_effects=True, vmem_limit_bytes=48 * 2**20
        ),
        name="gather_all",
    )(*blocks)


def hidden_units(gathered, whole_gate, whole_up):
    gate_rows = jnp.dot(gathered, whole_gate, preferred_element_type=jnp.float32)
    up_rows = jnp.dot(gathered, whole_up, preferred_element_type=jnp.float32)
    return (jax.nn.silu(gate_rows) * up_rows).astype(jnp.bfloat16)


def columns_of(blocks):
    return blocks.transpose(1, 0, 2).reshape(blocks.shape[1], -1)


def causal_taps(glu, kernel):
    length = glu.shape[0]
    taps = kernel.shape[0]
    padded = jnp.pad(glu, ((taps - 1, 0), (0, 0)))
    output = jnp.zeros_like(glu)
    for tap_index in range(taps):
        output = output + padded[tap_index : tap_index + length] * kernel[tap_index]
    return output


def chunked(block, pieces):
    return block.reshape(pieces, block.shape[0] // pieces, block.shape[1])


def shards(
    tokens,
    norm_first,
    norm_mixer,
    norm_second,
    ffn_gate,
    ffn_up,
    ffn_down,
    conv_value,
    conv_gate,
    depthwise,
    conv_gain,
    conv_out,
):
    width = tokens.shape[-1]
    stream = tokens.reshape(-1, width).astype(jnp.float32)
    first_rows = widen(rms_rows(stream, norm_first))
    small = jnp.concatenate([conv_value, conv_gate, conv_out.reshape(-1, conv_value.shape[1])])
    gate, up, down, small_all = gather_all(
        [chunked(ffn_gate, 4), chunked(ffn_up, 4), chunked(ffn_down, 4), chunked(small, 2)]
    )
    whole_gate = gate.reshape(-1, gate.shape[-1])
    whole_up = up.reshape(-1, up.shape[-1])
    whole_down = columns_of(down.reshape(down.shape[0], -1, down.shape[-1]))
    total = small_all.shape[0]
    small_all = small_all.reshape(total, -1, small_all.shape[-1])
    rows = conv_value.shape[0]
    channels_here = conv_value.shape[1]
    whole_value = small_all[:, :rows].reshape(-1, channels_here)
    whole_conv_gate = small_all[:, rows : 2 * rows].reshape(-1, channels_here)
    whole_out = columns_of(small_all[:, 2 * rows :].reshape(total, *conv_out.shape))

    hidden = hidden_units(first_rows, whole_gate, whole_up)
    stream = stream + 0.5 * narrow(jnp.dot(hidden, whole_down, preferred_element_type=jnp.float32))
    gathered = widen(rms_rows(stream, norm_mixer))
    values = jnp.dot(gathered, whole_value, preferred_element_type=jnp.float32)
    gates = jnp.dot(gathered, whole_conv_gate, preferred_element_type=jnp.float32)
    glu = reorder(values * jax.nn.sigmoid(gates))
    conv = causal_taps(glu, depthwise.astype(jnp.float32))
    channels = conv.shape[1] * lax.axis_size("tp")
    sums, squares = lax.psum((jnp.sum(conv, axis=1), jnp.sum(conv * conv, axis=1)), "tp")
    average = sums / channels
    spread = jnp.maximum(squares / channels - average * average, 0.0)
    centred = conv - average[:, None]
    activated = jax.nn.silu(
        centred * lax.rsqrt(spread[:, None] + CHAN_EPS) * conv_gain.astype(jnp.float32)
    ).astype(jnp.bfloat16)
    stream = stream + narrow(jnp.dot(reorder(activated), whole_out, preferred_element_type=jnp.float32))
    second_rows = widen(rms_rows(stream, norm_second))
    second_hidden = hidden_units(second_rows, whole_gate, whole_up)
    stream = stream + 0.5 * narrow(jnp.dot(second_hidden, whole_down, preferred_element_type=jnp.float32))
    return stream.astype(jnp.bfloat16).reshape(tokens.shape)


def solution(mesh):
    in_specs = (
        P(("rep", "fs"), "tp", None),
        P(),
        P(),
        P(),
        P("fs", "tp"),
        P("fs", "tp"),
        P("tp", "fs"),
        P("fs", "tp"),
        P("fs", "tp"),
        P(None, "tp"),
        P("tp"),
        P("tp", "fs"),
    )
    out_specs = P(("rep", "fs"), "tp", None)
    return jax.shard_map(shards, mesh=mesh, in_specs=in_specs, out_specs=out_specs, check_vma=False)
```

time: 537 us -> 411 us (0.77)
  waiting for transfers between devices: 451 us -> 9.58 us
  Pallas kernels: 0 us -> 319 us
  local copies, waits for them, and re-layouts: 0.53 us -> 15.9 us
  between operations: 13.7 us -> 0.32 us
  matrix products: 52.1 us -> 46.3 us
    all_gather x9 -> x0, waiting for transfers between devices: 420 us -> none  [the longest x1 95.7 us: shards(): lax.all_gather(ffn_gate, 'fs', axis=0, tiled=True)]
    pallas_call x0 -> x1, Pallas kernels: none -> 319 us  [gather_all(): pl.pallas_call(functools.partial(gather_kernel, total // 2, count), out_s...]
    reduce_scatter x3 -> x0, waiting for transfers between devices: 26.8 us -> none  [narrow(): lax.psum_scatter(partial_value.astype(jnp.bfloat16), 'tp', scatter_dimens...]
    ppermute x0 -> x6, waiting for transfers between devices: none -> 9.58 us  [swap(): return lax.ppermute(value, 'tp', [(i, size - 1 - i) for i in range(size)])]
    reshape x0 -> x1, local copies, waits for them, and re-layouts: none -> 8.26 us  [shards(): whole_down = columns_of(down.reshape(down.shape[0], -1, down.shape[-1]))]
    dot_general x6, matrix products: 38.2 us -> 32.7 us  [the longest x1 14 us: shards(): jnp.dot(hidden, whole_down, preferred_element_type=jnp.float32)]
  transfers between devices with their start and end apart: 12 -> 6, of which waited for: 12 -> 4; matrix products, arithmetic and copies ran while one was open for 4% -> 3% of each run, Pallas kernels for 0% -> 78%
where the time goes in v1:
time: 411 us; the launch traced here: 410 us
  Pallas kernels  319 us (78%)
  matrix products  46.3 us (11%)
  local copies, waits for them, and re-layouts  15.9 us (4%)
  other arithmetic  14.3 us (3%)
  waiting for transfers between devices  9.58 us (2%)
    pallas_call x1, Pallas kernels, gather_all(): pl.pallas_call(functools.partial(gather_kernel, total // 2, count), out_s...  319 us
    dot_general x1, matrix products, shards(): jnp.dot(hidden, whole_down, preferred_element_type=jnp.float32)  14 us
    dot_general x1, matrix products, shards(): jnp.dot(second_hidden, whole_down, preferred_element_type=jnp.float32)  13.7 us
    dot_general x2, matrix products, hidden_units(): up_rows = jnp.dot(gathered, whole_up, preferred_element_type=jnp.float32)  13.3 us
    ppermute x6, waiting for transfers between devices, swap(): return lax.ppermute(value, 'tp', [(i, size - 1 - i) for i in range(size)])  9.58 us
    reshape x1, local copies, waits for them, and re-layouts, shards(): whole_down = columns_of(down.reshape(down.shape[0], -1, down.shape[-1]))  8.26 us
  transfers between devices with their start and end apart: 6, of which 4 were waited for; matrix products, arithmetic and copies ran while one was open for 3% of the time, Pallas kernels for 78%

profile of v1, /device:TPU:0, one launch (start us, length us, event | category | flops | bytes accessed | tf_op | source)
XLA Modules:
  0.0 410.0 jit_solution(15881589800103331446)
XLA Ops:
  0.0 0.0 copy-start.2
  0.0 0.8 convert_element_type.73
  0.9 1.5 fusion
  2.4 2.5 fusion.2
  4.9 0.5 collective-permute-start
  5.4 0.0 copy-done.12
  5.4 0.0 copy-done.13
  5.4 0.0 copy-done.14
  5.4 0.0 copy-done
  5.4 0.0 copy-done.1
  5.5 0.0 copy-done.2
  5.5 319.2 %gather_all.1 = (bf16[8,4,64,1408]{3,2,1,0:T(8,128)(2,1)}, bf16[8,4,64,1408]{3,2,1,0:T(8,128)(2,1)}, bf16[8,4,352,256]{3,2,1,0:T(8,128)(2,1)}, bf16[8,2,384,256]{3,2,1,0:T(8,128)(2,1)S(1)}) custom-call(bf16[4,64,1408]{2,1,0:T(8,128)(2,1)S(1)} %bitcast.72, bf16[4,64,1408]{2,1,0:T(8,128)(2,1)S(1)} %bitcast.73, bf16[4,352,256]{2,1,0:T(8,128)(2,1)S(1)} %bitcast.74, ...), custom_call_target="tpu_custom_call" | custom-call | tf_op jit(solution)/shard_map/gather_all/pallas_call | solution.py:182
  324.6 8.3 %copy.13 = bf16[8,1408,256]{1,2,0:T(8,128)(2,1)} copy(bf16[8,1408,256]{2,1,0:T(8,128)(2,1)} %bitcast.77) | data formatting | bytes 11534336 | tf_op jit(solution)/shard_map/reshape | solution.py:244
  332.9 0.0 collective-permute-done
  332.9 8.3 %fusion.9 = f32[512,1408]{1,0:T(8,128)} fusion(bf16[2048,1408]{1,0:T(8,128)(2,1)} %bitcast.114, bf16[256,2048]{1,0:T(8,128)(2,1)} %collective-permute-done, bf16[256,2048]{1,0:T(8,128)(2,1)} %fusion.2), kind=kOutput, calls=%fused_computation.26 | convolution fusion | flops 2956984320 | bytes 10747904 | tf_op jit(solution)/shard_map/dot_general | solution.py:199
  341.2 14.0 %convolution_convert_fusion.2 = bf16[512,2048]{1,0:T(8,128)(2,1)} fusion(bf16[1408,2048]{0,1:T(8,128)(2,1)} %bitcast.75, f32[512,1408]{1,0:T(8,128)} %fusion.9, bf16[2048,1408]{1,0:T(8,128)(2,1)} %bitcast.112, bf16[256,2048]{1,0:T(8,128)(2,1)} %collective-permute-done, bf16[256,2048]{1,0:T(8,128)(2,1)} %fusion.2), kind=kOutput, calls=%fused_computation.5 | convolution fusion | flops 5915148288 | bytes 18612224 | tf_op jit(solution)/shard_map/dot_general | solution.py:254
  355.2 1.4 slice.298
  356.6 0.0 copy-start.7
  356.6 0.1 collective-permute-start.1
  356.7 0.0 copy-done.16
  356.7 2.6 collective-permute-done.1
  359.3 0.0 copy-done.3
  359.3 2.2 multiply_reduce_fusion.1
  361.6 0.0 copy-done.7
  361.6 1.7 multiply_convert_fusion.3
  363.3 0.0 copy-done.5
  363.3 0.1 collective-permute-start.2
  363.4 1.8 fusion.65
  365.2 1.7 copy.15
  367.0 0.0 copy-done.19
  367.0 0.0 copy-done.15
  367.1 0.0 collective-permute-done.2
  367.1 0.0 copy-done.11
  367.1 0.0 copy-start.10
  367.1 2.4 fusion.15
  369.5 0.0 copy-done.10
  369.5 2.3 fusion.11
  371.8 0.1 maximum_select_fusion
  371.9 2.4 fusion.64
  374.2 2.5 all-reduce.1
  376.8 0.2 multiply_convert_fusion.6
  377.0 0.0 copy-start.17
  377.0 0.0 copy-start.4
  377.1 0.0 copy-start.6
  377.1 0.0 copy-start.8
  377.1 0.8 convolution_convert_fusion
  377.8 0.1 slice.338
  377.9 0.4 collective-permute-start.3
  378.3 0.0 copy-done.17
  378.3 2.3 collective-permute-done.3
  380.6 0.0 copy-done.4
  380.6 0.0 copy-done.6
  380.7 1.0 multiply_reduce_fusion
  381.7 0.3 multiply_convert_fusion.2
  381.9 0.4 collective-permute-start.4
  382.3 2.3 collective-permute-done.4
  384.7 1.0 copy-done.18
  385.6 0.0 slice-done
  385.6 5.1 %fusion.5 = f32[512,1408]{1,0:T(8,128)} fusion(bf16[2048,1408]{1,0:T(8,128)(2,1)S(1)} %bitcast.117, bf16[256,2048]{1,0:T(8,128)(2,1)S(1)} %collective-permute-done.4, bf16[256,2048]{1,0:T(8,128)(2,1)S(1)} %multiply_convert_fusion.2), kind=kOutput, calls=%fused_computation.22 | convolution fusion | flops 2956984320 | bytes 10747904 | tf_op jit(solution)/shard_map/dot_general | solution.py:199
  390.7 13.7 %convolution_convert_fusion.1 = bf16[512,2048]{1,0:T(8,128)(2,1)} fusion(bf16[1408,2048]{0,1:T(8,128)(2,1)} %bitcast.76, f32[512,1408]{1,0:T(8,128)} %fusion.5, bf16[2048,1408]{1,0:T(8,128)(2,1)} %bitcast.113, bf16[256,2048]{1,0:T(8,128)(2,1)} %copy-done.18, bf16[256,2048]{1,0:T(8,128)(2,1)S(1)} %multiply_convert_fusion.2), kind=kOutput, calls=%fused_computation.4 | convolution fusion | flops 5915148288 | bytes 18612224 | tf_op jit(solution)/shard_map/dot_general | solution.py:271
  404.3 1.4 slice.340
  405.8 0.4 collective-permute-start.5
  406.2 2.3 collective-permute-done.5
  408.5 1.5 fusion.16
  (31 shorter events, 0.2 us)
Async XLA Ops:
  0.0 5.4 %copy-start.12 = (bf16[256,256]{1,0:T(8,128)(2,1)S(1)}, bf16[256,256]{1,0:T(8,128)(2,1)}, u32[]{:S(2)}) copy-start(bf16[256,256]{1,0:T(8,128)(2,1)} %param.23) | copy-start | bytes 393220
  0.0 5.4 %copy-start.13 = (bf16[256,256]{1,0:T(8,128)(2,1)S(1)}, bf16[256,256]{1,0:T(8,128)(2,1)}, u32[]{:S(2)}) copy-start(bf16[256,256]{1,0:T(8,128)(2,1)} %param.20) | copy-start | bytes 393220
  0.0 5.4 %copy-start.14 = (bf16[256,256]{1,0:T(8,128)(2,1)S(1)}, bf16[256,256]{1,0:T(8,128)(2,1)}, u32[]{:S(2)}) copy-start(bf16[256,256]{1,0:T(8,128)(2,1)} %param.19) | copy-start | bytes 393220
  0.0 5.4 %copy-start = (bf16[256,1408]{1,0:T(8,128)(2,1)S(1)}, bf16[256,1408]{1,0:T(8,128)(2,1)}, u32[]{:S(2)}) copy-start(bf16[256,1408]{1,0:T(8,128)(2,1)} %param.16) | copy-start | bytes 2162692
  0.0 5.4 %copy-start.1 = (bf16[256,1408]{1,0:T(8,128)(2,1)S(1)}, bf16[256,1408]{1,0:T(8,128)(2,1)}, u32[]{:S(2)}) copy-start(bf16[256,1408]{1,0:T(8,128)(2,1)} %param.17) | copy-start | bytes 2162692
  0.0 5.4 %copy-start.2 = (bf16[1408,256]{1,0:T(8,128)(2,1)S(1)}, bf16[1408,256]{1,0:T(8,128)(2,1)}, u32[]{:S(2)}) copy-start(bf16[1408,256]{1,0:T(8,128)(2,1)} %param.18) | copy-start | bytes 2162692
  4.9 328.0 %collective-permute-start = (bf16[256,2048]{1,0:T(8,128)(2,1)}, bf16[256,2048]{1,0:T(8,128)(2,1)}, u32[]{:S(2)}, u32[]{:S(2)}) collective-permute-start(bf16[256,2048]{1,0:T(8,128)(2,1)} %fusion.2), channel_id=1, source_target_pairs={{0,1},{1,0},{2,3},{3,2},{4,5},{5,4},{6,7},{7,6},{8,9},{9,8},{10,11... | collective-permute-start | bytes 3145736 | tf_op jit(solution)/shard_map/ppermute | solution.py:26
  355.2 1.5 copy-start.16
  355.2 4.1 %copy-start.3 = (bf16[1,256,2048]{2,1,0:T(8,128)(2,1)S(1)}, bf16[1,256,2048]{2,1,0:T(8,128)(2,1)}, u32[]{:S(2)}) copy-start(bf16[1,256,2048]{2,1,0:T(8,128)(2,1)} %param.12) | copy-start | bytes 3145732
  356.6 5.0 %copy-start.7 = (bf16[512,2048]{1,0:T(8,128)(2,1)S(1)}, bf16[512,2048]{1,0:T(8,128)(2,1)}, u32[]{:S(2)}) copy-start(bf16[512,2048]{1,0:T(8,128)(2,1)} %convolution_convert_fusion.2) | copy-start | bytes 6291460
  356.6 2.7 collective-permute-start.1
  359.3 3.9 copy-start.5
  363.3 3.8 collective-permute-start.2
  365.2 1.8 copy-start.19
  365.2 1.8 copy-start.15
  365.2 1.9 copy-start.11
  367.1 2.4 copy-start.10
  377.0 1.3 copy-start.17
  377.0 3.6 copy-start.4
  377.1 3.6 copy-start.6
  377.1 3.6 copy-start.8
  377.9 2.7 collective-permute-start.3
  378.3 7.3 %slice-start = ((s8[5767168]{0:T(1024)(128)(4,1)}), s8[4194304]{0:T(1024)(128)(4,1)S(1)}, s32[]{:S(2)}) async-start(s8[5767168]{0:T(1024)(128)(4,1)} %bitcast.115), calls=%async_computation | async-start | bytes 8388608
  378.3 7.3 %slice-start.1 = ((s8[5767168]{0:T(1024)(128)(4,1)}), s8[1572864]{0:T(1024)(128)(4,1)S(1)}, s32[]{:S(2)}) async-start(s8[5767168]{0:T(1024)(128)(4,1)} %bitcast.115), calls=%async_computation.1 | async-start | bytes 3145728
  381.9 2.7 collective-permute-start.4
  384.6 1.0 copy-start.18
  404.3 4.2 %copy-start.9 = (bf16[512,2048]{1,0:T(8,128)(2,1)S(1)}, bf16[512,2048]{1,0:T(8,128)(2,1)}, u32[]{:S(2)}) copy-start(bf16[512,2048]{1,0:T(8,128)(2,1)} %convolution_convert_fusion.1) | copy-start | bytes 6291460
  405.8 2.7 collective-permute-start.5
